TPU v7x, 32 devices: a whole 2x2x4 slice. The times are simulated.
32 devices in a mesh: grp: 2 (over y), sp: 4 (over z), tp: 4 (over x, core).
Axes of the slice: x: 2, y: 2, z: 4, core: 2. Of those that a mesh axis runs over, the one named last changes fastest.
Arguments:
- carryover_vector: bfloat16 [2048, 2048], P(('grp', 'sp', 'tp')), parts along dimension 0, may hold values from -6 to 6
- channel_source_entries: bfloat16 [2048, 1024], P(('grp', 'sp'), 'tp'), parts along dimension 0, may hold values from -6 to 6
- final_modulation_vector: bfloat16 [2048, 1024], P(('grp', 'sp'), 'tp'), parts along dimension 0, may hold values from -54 to 54
- entering_basis_matrix: bfloat16 [2048, 512], P(('grp', 'sp'), 'tp'), parts along dimension 0, may hold values from -6 to 6
- readout_basis_matrix: bfloat16 [2048, 512], P(('grp', 'sp'), 'tp'), parts along dimension 0, may hold values from -6 to 6
- raw_stride_amount: float32 [2048, 16], P(('grp', 'sp'), 'tp'), parts along dimension 0, may hold values from -6 to 5
- extra_log_attenuation: float32 [2048, 16], P(('grp', 'sp'), 'tp'), parts along dimension 0, may hold values from -1.4 to 0
- channel_fading_rate: float32 [16], P('tp'), may hold values from 0 to 0.1, as said below
- channel_source_kernel: float32 [4, 1024], P(None, 'tp'), may hold values from -3 to 3
- entering_basis_kernel: float32 [4, 512], P(None, 'tp'), may hold values from -3 to 3
- readout_basis_kernel: float32 [4, 512], P(None, 'tp'), may hold values from -3 to 3
- modulated_rescaling_vector: float32 [1024], replicated, may hold values from 0.1 to 1.9
- blender_final_matrix: bfloat16 [1024, 2048], replicated, may hold values from -0.1875 to 0.1875
- specialist_rescaling_vector: float32 [2048], replicated, may hold values from 0.1 to 1.9
- specialist_gating_matrices: bfloat16 [8, 2048, 1024], P('sp', None, 'tp'), may hold values from -0.125 to 0.125
- widening_matrices: bfloat16 [8, 2048, 1024], P('sp', None, 'tp'), may hold values from -0.125 to 0.125
- contracting_matrices: bfloat16 [8, 1024, 2048], P('sp', 'tp'), may hold values from -0.1875 to 0.1875
- assigned_specialist_ids: int32 [2048, 2], P(('grp', 'sp')), parts along dimension 0, may hold values from 0 to 7, as said below
- specialist_choice_affinity: float32 [2048, 2], P(('grp', 'sp', 'tp')), parts along dimension 0, may hold values from -6 to 6
- cluster_chance: float32 [2048], P(('grp', 'sp', 'tp')), parts along dimension 0, may hold values from 0.25 to 1
Outputs:
- layer_out: bfloat16 [2048, 2048], P(('grp', 'sp', 'tp')), parts along dimension 0
There are 2 independent parts, one for each index of `grp`. A program takes and returns all parts, laid end to end along the dimension named above; an argument that names none is the same for every part. Nothing has to cross between parts.
Inputs may be any that keep to these rules, and one draw needn't show every extreme that they name: `assigned_specialist_ids`: each row names 2 different experts of one group: the experts g * 2 to (g + 1) * 2 - 1 for one g below 4. In each aligned block of 64 rows (the rows of one device) no expert is named by more than 32 rows, and every expert of one group, the same group in all blocks, is named by exactly 32 rows of every block. `channel_fading_rate`: positive.
All inputs are finite; a program needn't handle non-finite values.
Results may differ from a plain program's by a relative error of at most 0.015.
Values may be sent and summed in bfloat16 or wider, within the bound.
A program may use at most 64 MiB of HBM per device.

v0:
```python
import jax
import jax.numpy as jnp
from jax import lax
from jax.sharding import PartitionSpec as P

HEAD_DIM = 64
STATE = 128
BLOCK = 64
EPS = 1e-06
HIGHEST = lax.Precision.HIGHEST


def prefix(x, axis, combine, identity):
    size, index = (lax.axis_size(axis), lax.axis_index(axis))
    everything = jax.tree.map(
        lambda part, kind: lax.all_gather(part.astype(kind), axis), x, (jnp.bfloat16, jnp.bfloat16)
    )
    start = jax.tree.map(
        lambda part, zero: jnp.broadcast_to(jnp.asarray(zero, part.dtype), part.shape), x, identity
    )

    def lap(k, before):
        reached = k < index
        new = combine(
            before, jax.tree.map(lambda part, own: part[k].astype(own.dtype), everything, x)
        )
        return jax.tree.map(lambda a, b: jnp.where(reached, a, b), new, before)

    return lax.fori_loop(0, size, lap, start)


def from_behind(x, axis, by):
    size = lax.axis_size(axis)
    pairs = [(i, i + by) for i in range(size) if 0 <= i + by < size]
    return lax.ppermute(x, axis, pairs)


def causal_conv(signal, earlier, weights):
    kernel_len = weights.shape[0]
    length = signal.shape[0]
    joined = jnp.concatenate([earlier, signal], axis=0).astype(jnp.float32)
    accumulated = jnp.zeros((length, signal.shape[1]), jnp.float32)
    for offset in range(kernel_len):
        accumulated = accumulated + weights[offset][None, :] * joined[offset : offset + length]
    return jax.nn.silu(accumulated)


def link_states(earlier, later):
    return (earlier[0] * later[0], earlier[1] * later[0][..., None, None] + later[1])


def device_states(scaled_in, log_attenuation, keys_b, queries_c, groups_here):
    length = scaled_in.shape[0]
    blocks = length // BLOCK
    per_group = scaled_in.shape[1] // groups_here
    scaled_in = scaled_in.reshape(blocks, BLOCK, groups_here, per_group, HEAD_DIM)
    log_attenuation = log_attenuation.reshape(blocks, BLOCK, groups_here, per_group)
    keys_b = keys_b.reshape(blocks, BLOCK, groups_here, STATE)
    queries_c = queries_c.reshape(blocks, BLOCK, groups_here, STATE)
    running = jnp.cumsum(log_attenuation, axis=1)
    lower_mask = jnp.tril(jnp.ones((BLOCK, BLOCK), dtype=bool))
    between = running[:, :, None] - running[:, None, :]
    decays = jnp.exp(jnp.where(lower_mask[None, :, :, None, None], between, -jnp.inf))
    scores = jnp.einsum("blgn,bsgn->blsg", queries_c, keys_b, precision=HIGHEST)
    inside = jnp.einsum("blsg,blsgr,bsgrp->blgrp", scores, decays, scaled_in, precision=HIGHEST)
    totals = running[:, -1]
    remain = jnp.exp(totals[:, None] - running)
    block_states = jnp.einsum(
        "bsgn,bsgr,bsgrp->bgrpn", keys_b, remain, scaled_in, precision=HIGHEST
    )

    def advance(carried, pieces):
        return (carried * jnp.exp(pieces[1])[..., None, None] + pieces[0], carried)

    initial = jnp.zeros(block_states.shape[1:], jnp.float32)
    own_state, entering = lax.scan(advance, initial, (block_states, totals))
    own_decay = jnp.exp(jnp.sum(totals, axis=0))
    _, incoming = prefix(
        (own_decay, own_state),
        "sp",
        link_states,
        (jnp.ones_like(own_decay), jnp.zeros_like(own_state)),
    )
    preceding = jnp.exp(jnp.cumsum(totals, axis=0) - totals)
    entering = entering + preceding[..., None, None] * incoming[None]
    outside = jnp.einsum(
        "blgn,bgrpn,blgr->blgrp", queries_c, entering, jnp.exp(running), precision=HIGHEST
    )
    return (inside + outside).reshape(length, -1)


def fetch_rows(tokens, sources):
    present = sources >= 0
    picked = jnp.take(tokens, jnp.maximum(sources, 0), axis=0)
    return jnp.where(present[:, None], picked, jnp.zeros_like(picked))


def slot_tables(chosen_ids, quarters, row_count, experts, capacity):
    picks = chosen_ids.shape[1]
    flat_ids = chosen_ids.reshape(quarters, row_count * picks)
    member = (flat_ids[..., None] == jnp.arange(experts, dtype=jnp.int32)).astype(jnp.int32)
    position = jnp.sum((jnp.cumsum(member, axis=1) - member) * member, axis=2)
    quarter_ids = jnp.arange(quarters, dtype=jnp.int32)[:, None]
    slot_index = flat_ids * (quarters * capacity) + quarter_ids * capacity + position
    token_index = (
        quarter_ids * row_count + jnp.arange(row_count * picks, dtype=jnp.int32)[None, :] // picks
    )
    sources = (
        jnp.full((experts * quarters * capacity,), -1, jnp.int32)
        .at[slot_index.reshape(-1)]
        .set(token_index.reshape(-1))
    )
    return (sources, position)


def per_device(
    carryover_vector,
    channel_source_entries,
    final_modulation_vector,
    entering_basis_matrix,
    readout_basis_matrix,
    raw_stride_amount,
    extra_log_attenuation,
    channel_fading_rate,
    channel_source_kernel,
    entering_basis_kernel,
    readout_basis_kernel,
    modulated_rescaling_vector,
    blender_final_matrix,
    specialist_rescaling_vector,
    specialist_gating_matrices,
    widening_matrices,
    contracting_matrices,
    assigned_specialist_ids,
    specialist_choice_affinity,
    cluster_chance,
):
    length = channel_source_entries.shape[0]
    row_count = carryover_vector.shape[0]
    model_width = carryover_vector.shape[1]
    heads_here = channel_fading_rate.shape[0]
    groups_here = entering_basis_matrix.shape[1] // STATE
    tp_index = lax.axis_index("tp")
    rim_rows = channel_source_kernel.shape[0] - 1
    neighbours = from_behind(
        (
            channel_source_entries[length - rim_rows :],
            entering_basis_matrix[length - rim_rows :],
            readout_basis_matrix[length - rim_rows :],
        ),
        "sp",
        1,
    )
    inputs_x = causal_conv(channel_source_entries, neighbours[0], channel_source_kernel)
    keys_b = causal_conv(entering_basis_matrix, neighbours[1], entering_basis_kernel)
    queries_c = causal_conv(readout_basis_matrix, neighbours[2], readout_basis_kernel)
    channel_stride_amount = jax.nn.softplus(raw_stride_amount)
    log_attenuation = extra_log_attenuation - channel_fading_rate[None, :] * channel_stride_amount
    heads_x = inputs_x.reshape(length, heads_here, HEAD_DIM)
    mixed = device_states(
        heads_x * channel_stride_amount[:, :, None], log_attenuation, keys_b, queries_c, groups_here
    )
    gated = mixed * jax.nn.silu(final_modulation_vector.astype(jnp.float32))
    head_cols = gated.shape[1]
    squares = lax.psum(jnp.sum(gated * gated, axis=1), "tp")
    first_col = tp_index * head_cols
    gain_part = lax.dynamic_slice_in_dim(modulated_rescaling_vector, first_col, head_cols, 0)
    scale = lax.rsqrt(squares / (head_cols * lax.axis_size("tp")) + EPS)
    normed = (gated * scale[:, None] * gain_part[None, :]).astype(jnp.bfloat16)
    weight_rows = lax.dynamic_slice_in_dim(blender_final_matrix, first_col, head_cols, 0)
    summed = lax.psum_scatter(
        jnp.dot(normed, weight_rows, preferred_element_type=jnp.float32).astype(jnp.bfloat16),
        "tp",
        scatter_dimension=0,
        tiled=True,
    ).astype(jnp.float32)
    middle = (carryover_vector.astype(jnp.float32) + summed).astype(jnp.bfloat16)
    middle_wide = middle.astype(jnp.float32)
    expert_input = (
        middle_wide
        * lax.rsqrt(jnp.mean(middle_wide * middle_wide, axis=1, keepdims=True) + EPS)
        * specialist_rescaling_vector[None, :]
    ).astype(jnp.bfloat16)
    sp_count = lax.axis_size("sp")
    local_experts = specialist_gating_matrices.shape[0]
    experts = sp_count * local_experts
    picks = assigned_specialist_ids.shape[1]
    capacity = 2 * row_count * picks // experts
    own_ids = lax.dynamic_slice_in_dim(assigned_specialist_ids, tp_index * row_count, row_count, 0)
    sources, position = slot_tables(own_ids, 1, row_count, experts, capacity)
    own_position = position[0]
    outgoing = fetch_rows(expert_input, sources).reshape(
        sp_count, local_experts, 1, capacity, model_width
    )
    received = lax.all_to_all(outgoing, "sp", split_axis=0, concat_axis=0, tiled=True)
    arrived = lax.all_gather(received, "tp", axis=2, tiled=True)
    gate_value = jnp.einsum(
        "slqcd,ldf->slqcf", arrived, specialist_gating_matrices, preferred_element_type=jnp.float32
    )
    up_value = jnp.einsum(
        "slqcd,ldf->slqcf", arrived, widening_matrices, preferred_element_type=jnp.float32
    )
    hidden = (jax.nn.silu(gate_value) * up_value).astype(jnp.bfloat16)
    partial_value = jnp.einsum(
        "slqcf,lfd->slqcd", hidden, contracting_matrices, preferred_element_type=jnp.float32
    )
    width_total = lax.psum_scatter(
        partial_value.astype(jnp.bfloat16), "tp", scatter_dimension=2, tiled=True
    )
    returned = lax.all_to_all(width_total, "sp", split_axis=0, concat_axis=0, tiled=True)
    answers = returned.reshape(experts * capacity, model_width)
    own_slots = own_ids.reshape(-1) * capacity + own_position
    gathered = (
        jnp.take(answers, own_slots, axis=0)
        .reshape(row_count, picks, model_width)
        .astype(jnp.float32)
    )
    lifted = jnp.exp(specialist_choice_affinity)
    shares = cluster_chance[:, None] * lifted / jnp.sum(lifted, axis=1, keepdims=True)
    return (middle_wide + jnp.sum(shares[:, :, None] * gathered, axis=1)).astype(jnp.bfloat16)


def solution(mesh):
    return jax.shard_map(
        per_device,
        mesh=mesh,
        in_specs=(
            P(("grp", "sp", "tp"), None),
            P(("grp", "sp"), "tp"),
            P(("grp", "sp"), "tp"),
            P(("grp", "sp"), "tp"),
            P(("grp", "sp"), "tp"),
            P(("grp", "sp"), "tp"),
            P(("grp", "sp"), "tp"),
            P("tp"),
            P(None, "tp"),
            P(None, "tp"),
            P(None, "tp"),
            P(),
            P(),
            P(),
            P("sp", None, "tp"),
            P("sp", None, "tp"),
            P("sp", "tp", None),
            P(("grp", "sp"), None),
            P(("grp", "sp", "tp"), None),
            P(("grp", "sp", "tp")),
        ),
        out_specs=P(("grp", "sp", "tp"), None),
        check_vma=False,
    )
```

profile of v0, /device:TPU:0, one launch (start us, length us, event | category | flops | bytes accessed | tf_op | source)
XLA Modules:
  0.0 319.8 jit_solution(16256433366509483427)
XLA Ops:
  7.4 4.9 %collective-permute-start.2 = (bf16[3,256]{1,0:T(4,128)(2,1)S(1)}, bf16[3,256]{1,0:T(4,128)(2,1)S(1)}, u32[]{:S(2)}, u32[]{:S(2)}) collective-permute-start(bf16[3,256]{1,0:T(4,128)(2,1)S(1)} %slice.103), channel_id=1, source_target_pairs={{0,4},{4,8},{8,12},{1,5},{5,9},{9,13},{2,6},{6,10},{10,14},{3,7},{... | collective-permute-start | bytes 4616 | tf_op jit(solution)/shard_map/ppermute | solution.py:35
  13.0 3.5 %collective-permute-start = (bf16[3,128]{1,0:T(4,128)(2,1)S(1)}, bf16[3,128]{1,0:T(4,128)(2,1)S(1)}, u32[]{:S(2)}, u32[]{:S(2)}) collective-permute-start(bf16[3,128]{1,0:T(4,128)(2,1)S(1)} %slice.85), channel_id=1, source_target_pairs={{0,4},{4,8},{8,12},{1,5},{5,9},{9,13},{2,6},{6,10},{10,14},{3,7},{... | collective-permute-start | bytes 2312 | tf_op jit(solution)/shard_map/ppermute | solution.py:35
  17.2 3.5 %collective-permute-start.1 = (bf16[3,128]{1,0:T(4,128)(2,1)S(1)}, bf16[3,128]{1,0:T(4,128)(2,1)S(1)}, u32[]{:S(2)}, u32[]{:S(2)}) collective-permute-start(bf16[3,128]{1,0:T(4,128)(2,1)S(1)} %slice.94), channel_id=1, source_target_pairs={{0,4},{4,8},{8,12},{1,5},{5,9},{9,13},{2,6},{6,10},{10,14},{3,7},{... | collective-permute-start | bytes 2312 | tf_op jit(solution)/shard_map/ppermute | solution.py:35
  25.5 1.2 dynamic-slice
  27.7 8.4 %all-reduce = bf16[16]{0:T(256)(128)(2,1)S(1)} all-reduce(bf16[16]{0:T(256)(128)(2,1)S(1)} %dynamic-update-slice), channel_id=2, replica_groups=mesh['grp'=2,'sp'=4,'tp'=4] {'sp'}, use_global_device_ids=true, to_apply=%add | all-reduce | flops 16 | bytes 64
  38.8 1.3 dynamic_slice.31
  44.8 1.5 convolution_bitcast_fusion
  46.4 5.6 %while.27 = (s32[]{:T(128)}, f32[1,4,64,128]{3,2,1,0:T(8,128)S(1)}, f32[4,1,4,64,128]{4,3,2,1,0:T(8,128)}, f32[4,1,4]{2,1,0:T(1,128)}, f32[4,1,4,64,128]{4,3,2,1,0:T(8,128)S(1)}, /*index=5*/s32[]{:T(128)}, s32[]{:T(128)}) while((s32[]{:T(128)}, f32[1,4,64,128]{3,2,1,0:T(8,128)S(1)}, f32[4,1,4,64,128]{4,3,2,1,0:T(8,128)}, ...), condition=%wide.region_2.3_spmd.clone, body=%wide.region_1.2_spmd.clone.sunk | while | flops 131075 | bytes 656016 | solution.py:76
  52.0 13.9 %all-gather.1 = bf16[4,4,64,128]{3,2,1,0:T(8,128)(2,1)S(1)} all-gather(bf16[1,4,64,128]{3,2,1,0:T(8,128)(2,1)S(1)} %convert_element_type.121), channel_id=3, replica_groups=mesh['grp'=2,'sp'=4,'tp'=4] {'sp'}, dimensions={0}, use_global_device_ids=true | all-gather | bytes 327680 | tf_op jit(solution)/shard_map/all_gather | solution.py:16
  66.0 3.0 while.28
  68.9 2.8 fusion.20
  71.7 2.0 fusion.21
  74.6 5.7 %psum.7 = f32[256]{0:T(256)S(1)} all-reduce(f32[256]{0:T(256)S(1)} %multiply_reduce_fusion.1), channel_id=1, replica_groups=mesh['grp'=2,'sp'=4,'tp'=4] {'tp'}, use_global_device_ids=true, to_apply=%region_8.9 | all-reduce | flops 256 | bytes 2048 | tf_op jit(solution)/shard_map/psum | solution.py:165
  80.3 2.7 convolution_convert_fusion
  85.3 22.6 %reduce-scatter.5.cloned.1.call-done = bf16[64,2048]{1,0:T(8,128)(2,1)} async-done(((bf16[256,2048]{1,0:T(8,128)(2,1)}), bf16[64,2048]{1,0:T(8,128)(2,1)}) %reduce-scatter.5.cloned.1.call-update) | async-done | bytes 262160 | tf_op jit(solution)/shard_map/reduce_scatter | solution.py:171
  108.0 1.1 fusion.25
  109.1 1.1 fusion.27
  110.2 1.4 gather_fusion
  111.8 30.0 %all_to_all.10 = bf16[4,2,1,32,2048]{4,3,2,1,0:T(8,128)(2,1)S(1)} all-to-all(bf16[4,2,1,32,2048]{4,3,2,1,0:T(8,128)(2,1)S(1)} %select_bitcast_fusion), channel_id=1, replica_groups=mesh['grp'=2,'sp'=4,'tp'=4] {'sp'}, dimensions={0} | all-to-all | bytes 2097152 | tf_op jit(solution)/shard_map/all_to_all | solution.py:195
  141.8 1.0 copy.93
  143.1 32.5 %all-gather.4.cloned.1.call-done = bf16[4,2,4,32,2048]{4,3,2,0,1:T(8,128)(2,1)} async-done(((bf16[4,2,1,32,2048]{4,3,2,0,1:T(8,128)(2,1)}), bf16[4,2,4,32,2048]{4,3,2,0,1:T(8,128)(2,1)}) %all-gather.4.cloned.1.call-update) | async-done | bytes 4194320 | tf_op jit(solution)/shard_map/all_gather | solution.py:196
  175.6 4.1 %fusion.8 = f32[4,2,4,32,256]{4,3,2,0,1:T(8,128)S(1)} fusion(bf16[4,2,4,32,2048]{4,3,2,0,1:T(8,128)(2,1)} %all-gather.4.cloned.1.call-done, bf16[2,2048,256]{2,1,0:T(8,128)(2,1)} %param.38), kind=kOutput, calls=%fused_computation.18 | convolution fusion | flops 1073741824 | bytes 7340032 | tf_op jit(solution)/shard_map/slqcd,ldf->slqcf/dot_general | solution.py:197
  179.7 7.3 %convert_bitcast_fusion = bf16[4,2,4,32,2048]{4,3,2,0,1:T(8,128)(2,1)} fusion(bf16[2,256,2048]{2,1,0:T(8,128)(2,1)S(1)} %copy-done, bf16[4,2,4,32,2048]{4,3,2,0,1:T(8,128)(2,1)} %all-gather.4.cloned.1.call-done, bf16[2,2048,256]{2,1,0:T(8,128)(2,1)} %param.39, f32[4,2,4,32,256]{4,3,2,0,1:T(8,128)S(1)} %fusion.8), kind=kOutput, calls=%fused_computation.11 | convolution fusion | flops 2151153664 | bytes 13631488 | tf_op jit(solution)/shard_map/slqcf,lfd->slqcd/dot_general | solution.py:204
  188.3 84.4 %all-reduce.4.cloned.1.call-done = bf16[4,2,4,32,2048]{4,3,2,0,1:T(8,128)(2,1)} async-done(((bf16[4,2,4,32,2048]{4,3,2,0,1:T(8,128)(2,1)}), bf16[4,2,4,32,2048]{4,3,2,0,1:T(8,128)(2,1)}) %all-reduce.4.cloned.1.call-update) | async-done | bytes 4194320
  272.7 1.9 constant_dynamic-slice_fusion.1
  274.6 1.1 copy.94
  275.7 4.7 %all-to-all-start.1 = ((bf16[4,2,1,32,2048]{4,3,2,1,0:T(8,128)(2,1)}), bf16[4,2,1,32,2048]{4,3,2,1,0:T(8,128)(2,1)S(1)}, u32[]{:S(2)}, u32[]{:S(2)}) async-start(bf16[4,2,1,32,2048]{4,3,2,1,0:T(8,128)(2,1)} %copy.94), calls=%async_computation.2 | async-start | bytes 2097152 | tf_op jit(solution)/shard_map/all_to_all | solution.py:210
  280.9 24.9 %all-to-all-done.1 = bf16[4,2,1,32,2048]{4,3,2,1,0:T(8,128)(2,1)S(1)} async-done(((bf16[4,2,1,32,2048]{4,3,2,1,0:T(8,128)(2,1)}), bf16[4,2,1,32,2048]{4,3,2,1,0:T(8,128)(2,1)S(1)}, u32[]{:S(2)}, u32[]{:S(2)}) %all-to-all-start.1) | async-done | bytes 1048608 | tf_op jit(solution)/shard_map/all_to_all | solution.py:210
  305.8 1.7 gather_fusion.1
  307.5 1.4 gather.15
  308.9 2.5 multiply_reduce_fusion
  311.5 1.8 fusion.28
  (119 shorter events, 28.3 us)
Async XLA Ops:
  6.5 173.2 %copy-start = (bf16[2,256,2048]{2,1,0:T(8,128)(2,1)S(1)}, bf16[2,256,2048]{2,1,0:T(8,128)(2,1)}, u32[]{:S(2)}) copy-start(bf16[2,256,2048]{2,1,0:T(8,128)(2,1)} %param.40) | copy-start | bytes 6291460
  6.5 101.4 %reduce-scatter.5.cloned.1.call-start = ((), (), s32[]{:S(2)}) async-start(), calls=%async_computation.3 | async-start | bytes 1310720 | tf_op jit(solution)/shard_map/reduce_scatter | solution.py:171
  7.4 35.9 %collective-permute-start.2 = (bf16[3,256]{1,0:T(4,128)(2,1)S(1)}, bf16[3,256]{1,0:T(4,128)(2,1)S(1)}, u32[]{:S(2)}, u32[]{:S(2)}) collective-permute-start(bf16[3,256]{1,0:T(4,128)(2,1)S(1)} %slice.103), channel_id=1, source_target_pairs={{0,4},{4,8},{8,12},{1,5},{5,9},{9,13},{2,6},{6,10},{10,14},{3,7},{... | collective-permute-start | bytes 4616 | tf_op jit(solution)/shard_map/ppermute | solution.py:35
  13.0 27.1 %collective-permute-start = (bf16[3,128]{1,0:T(4,128)(2,1)S(1)}, bf16[3,128]{1,0:T(4,128)(2,1)S(1)}, u32[]{:S(2)}, u32[]{:S(2)}) collective-permute-start(bf16[3,128]{1,0:T(4,128)(2,1)S(1)} %slice.85), channel_id=1, source_target_pairs={{0,4},{4,8},{8,12},{1,5},{5,9},{9,13},{2,6},{6,10},{10,14},{3,7},{... | collective-permute-start | bytes 2312 | tf_op jit(solution)/shard_map/ppermute | solution.py:35
  17.2 24.0 %collective-permute-start.1 = (bf16[3,128]{1,0:T(4,128)(2,1)S(1)}, bf16[3,128]{1,0:T(4,128)(2,1)S(1)}, u32[]{:S(2)}, u32[]{:S(2)}) collective-permute-start(bf16[3,128]{1,0:T(4,128)(2,1)S(1)} %slice.94), channel_id=1, source_target_pairs={{0,4},{4,8},{8,12},{1,5},{5,9},{9,13},{2,6},{6,10},{10,14},{3,7},{... | collective-permute-start | bytes 2312 | tf_op jit(solution)/shard_map/ppermute | solution.py:35
  41.1 1.0 copy-start.3
  52.0 22.5 %copy-start.4 = (bf16[256,256]{1,0:T(8,128)(2,1)S(1)}, bf16[256,256]{1,0:T(8,128)(2,1)}, u32[]{:S(2)}) copy-start(bf16[256,256]{1,0:T(8,128)(2,1)} %param.26) | copy-start | bytes 393220
  52.0 28.3 %copy-start.7 = (f32[256]{0:T(256)S(1)}, f32[256]{0:T(256)}, u32[]{:S(2)}) copy-start(f32[256]{0:T(256)} %dynamic_slice.31) | copy-start | bytes 3076
  68.9 14.2 %copy-start.8 = (s32[256,2]{0,1:T(2,128)S(1)}, s32[256,2]{0,1:T(2,128)}, u32[]{:S(2)}) copy-start(s32[256,2]{0,1:T(2,128)} %param.41) | copy-start | bytes 6148
  71.7 36.3 %copy-start.1 = (bf16[64,2048]{1,0:T(8,128)(2,1)S(1)}, bf16[64,2048]{1,0:T(8,128)(2,1)}, u32[]{:S(2)}) copy-start(bf16[64,2048]{1,0:T(8,128)(2,1)} %param.24) | copy-start | bytes 786436
  71.7 37.4 %copy-start.5 = (f32[2048]{0:T(1024)S(1)}, f32[2048]{0:T(1024)}, u32[]{:S(2)}) copy-start(f32[2048]{0:T(1024)} %param.37) | copy-start | bytes 24580
  83.1 92.5 %all-gather.4.cloned.1.call-start = ((), (), s32[]{:S(2)}) async-start(), calls=%async_computation.4 | async-start | bytes 5242880 | tf_op jit(solution)/shard_map/all_gather | solution.py:196
  142.8 129.8 %all-reduce.4.cloned.1.call-start = ((), (), s32[]{:S(2)}) async-start(), calls=%async_computation.5 | async-start | bytes 8388608
  187.0 0.7 copy-start.10
  187.0 93.7 %copy-start.6 = (f32[64,2]{0,1:T(2,128)S(1)}, f32[64,2]{0,1:T(2,128)}, u32[]{:S(2)}) copy-start(f32[64,2]{0,1:T(2,128)} %param.42) | copy-start | bytes 1540
  187.1 93.7 %copy-start.9 = (f32[64]{0:T(128)S(1)}, f32[64]{0:T(128)}, u32[]{:S(2)}) copy-start(f32[64]{0:T(128)} %param.43) | copy-start | bytes 772
  275.7 35.8 %copy-start.2 = (bf16[64,2048]{1,0:T(8,128)(2,1)S(1)}, bf16[64,2048]{1,0:T(8,128)(2,1)}, u32[]{:S(2)}) copy-start(bf16[64,2048]{1,0:T(8,128)(2,1)} %param.24) | copy-start | bytes 786436
  275.7 30.1 %all-to-all-start.1 = ((bf16[4,2,1,32,2048]{4,3,2,1,0:T(8,128)(2,1)}), bf16[4,2,1,32,2048]{4,3,2,1,0:T(8,128)(2,1)S(1)}, u32[]{:S(2)}, u32[]{:S(2)}) async-start(bf16[4,2,1,32,2048]{4,3,2,1,0:T(8,128)(2,1)} %copy.94), calls=%async_computation.2 | async-start | bytes 2097152 | tf_op jit(solution)/shard_map/all_to_all | solution.py:210
Sparse Core Ops, SparseCore 0:
  83.2 24.7 reduce-scatter.4
  143.0 32.5 all-gather.3
  187.2 85.4 all-reduce.3
where the time goes:
time: 321 us; the launch traced here: 320 us
  waiting for transfers between devices  165 us (51%)
  blocking collectives  57.9 us (18%)
  local copies, waits for them, and re-layouts  26.1 us (8%)
  matrix products  20.8 us (6%)
  other arithmetic  19.1 us (6%)
  starting transfers between devices  16.9 us (5%)
  between operations  14.2 us (4%)
    unnamed x4, waiting for transfers between devices  84.5 us
    all_gather x1, waiting for transfers between devices, per_device(): arrived = lax.all_gather(received, 'tp', axis=2, tiled=True)  32.5 us
    all_to_all x1, blocking collectives, per_device(): lax.all_to_all(outgoing, 'sp', split_axis=0, concat_axis=0, tiled=True)  30 us
    all_to_all x1, waiting for transfers between devices, per_device(): lax.all_to_all(width_total, 'sp', split_axis=0, concat_axis=0, tiled=True)  24.9 us
    reduce_scatter x1, waiting for transfers between devices, per_device(): lax.psum_scatter(jnp.dot(normed, weight_rows, preferred_element_type=jnp....  22.6 us
    all_gather x1, blocking collectives, prefix(): lax.all_gather(part.astype(kind), axis)  13.9 us
    ppermute x3, starting transfers between devices, from_behind(): return lax.ppermute(x, axis, pairs)  11.9 us
    unnamed x1, blocking collectives  8.36 us
  transfers between devices with their start and end apart: 7, of which 4 were waited for; matrix products, arithmetic and copies ran while one was open for 6% of the time, Pallas kernels for 0%

commit v1 on v0

--- a/solution.py
+++ b/solution.py
@@ -193,7 +193,8 @@
         sp_count, local_experts, 1, capacity, model_width
     )
     received = lax.all_to_all(outgoing, "sp", split_axis=0, concat_axis=0, tiled=True)
-    arrived = lax.all_gather(received, "tp", axis=2, tiled=True)
+    tiles = lax.all_gather(received, "tp")
+    arrived = jnp.concatenate(tiles, axis=2)
     gate_value = jnp.einsum(
         "slqcd,ldf->slqcf", arrived, specialist_gating_matrices, preferred_element_type=jnp.float32
     )

time: 321 us -> 320 us (level)
  no operation moved by 1% of the time
where the time goes in v1:
time: 320 us; the launch traced here: 319 us
  waiting for transfers between devices  165 us (52%)
  blocking collectives  58 us (18%)
  local copies, waits for them, and re-layouts  25 us (8%)
  matrix products  20.8 us (6%)
  other arithmetic  19.1 us (6%)
  starting transfers between devices  16.9 us (5%)
  between operations  14.2 us (4%)
    unnamed x4, waiting for transfers between devices  84.5 us
    all_gather x1, waiting for transfers between devices, per_device(): tiles = lax.all_gather(received, 'tp')  32.5 us
    all_to_all x1, blocking collectives, per_device(): lax.all_to_all(outgoing, 'sp', split_axis=0, concat_axis=0, tiled=True)  30.1 us
    all_to_all x1, waiting for transfers between devices, per_device(): lax.all_to_all(width_total, 'sp', split_axis=0, concat_axis=0, tiled=True)  24.9 us
    reduce_scatter x1, waiting for transfers between devices, per_device(): lax.psum_scatter(jnp.dot(normed, weight_rows, preferred_element_type=jnp....  22.6 us
    all_gather x1, blocking collectives, prefix(): lax.all_gather(part.astype(kind), axis)  13.9 us
    ppermute x3, starting transfers between devices, from_behind(): return lax.ppermute(x, axis, pairs)  11.9 us
    unnamed x1, blocking collectives  8.36 us
  transfers between devices with their start and end apart: 7, of which 4 were waited for; matrix products, arithmetic and copies ran while one was open for 6% of the time, Pallas kernels for 0%

profile of v1, /device:TPU:0, one launch (start us, length us, event | category | flops | bytes accessed | tf_op | source)
XLA Modules:
  0.0 318.8 jit_solution(6473657620886182021)
XLA Ops:
  7.4 4.9 %collective-permute-start.2 = (bf16[3,256]{1,0:T(4,128)(2,1)S(1)}, bf16[3,256]{1,0:T(4,128)(2,1)S(1)}, u32[]{:S(2)}, u32[]{:S(2)}) collective-permute-start(bf16[3,256]{1,0:T(4,128)(2,1)S(1)} %slice.103), channel_id=1, source_target_pairs={{0,4},{4,8},{8,12},{1,5},{5,9},{9,13},{2,6},{6,10},{10,14},{3,7},{... | collective-permute-start | bytes 4616 | tf_op jit(solution)/shard_map/ppermute | solution.py:35
  13.0 3.5 %collective-permute-start = (bf16[3,128]{1,0:T(4,128)(2,1)S(1)}, bf16[3,128]{1,0:T(4,128)(2,1)S(1)}, u32[]{:S(2)}, u32[]{:S(2)}) collective-permute-start(bf16[3,128]{1,0:T(4,128)(2,1)S(1)} %slice.85), channel_id=1, source_target_pairs={{0,4},{4,8},{8,12},{1,5},{5,9},{9,13},{2,6},{6,10},{10,14},{3,7},{... | collective-permute-start | bytes 2312 | tf_op jit(solution)/shard_map/ppermute | solution.py:35
  17.2 3.5 %collective-permute-start.1 = (bf16[3,128]{1,0:T(4,128)(2,1)S(1)}, bf16[3,128]{1,0:T(4,128)(2,1)S(1)}, u32[]{:S(2)}, u32[]{:S(2)}) collective-permute-start(bf16[3,128]{1,0:T(4,128)(2,1)S(1)} %slice.94), channel_id=1, source_target_pairs={{0,4},{4,8},{8,12},{1,5},{5,9},{9,13},{2,6},{6,10},{10,14},{3,7},{... | collective-permute-start | bytes 2312 | tf_op jit(solution)/shard_map/ppermute | solution.py:35
  25.5 1.2 dynamic-slice
  27.7 8.4 %all-reduce = bf16[16]{0:T(256)(128)(2,1)S(1)} all-reduce(bf16[16]{0:T(256)(128)(2,1)S(1)} %dynamic-update-slice), channel_id=2, replica_groups=mesh['grp'=2,'sp'=4,'tp'=4] {'sp'}, use_global_device_ids=true, to_apply=%add | all-reduce | flops 16 | bytes 64
  38.8 1.3 dynamic_slice.31
  44.8 1.5 convolution_bitcast_fusion
  46.4 5.6 %while.27 = (s32[]{:T(128)}, f32[1,4,64,128]{3,2,1,0:T(8,128)S(1)}, f32[4,1,4,64,128]{4,3,2,1,0:T(8,128)}, f32[4,1,4]{2,1,0:T(1,128)}, f32[4,1,4,64,128]{4,3,2,1,0:T(8,128)S(1)}, /*index=5*/s32[]{:T(128)}, s32[]{:T(128)}) while((s32[]{:T(128)}, f32[1,4,64,128]{3,2,1,0:T(8,128)S(1)}, f32[4,1,4,64,128]{4,3,2,1,0:T(8,128)}, ...), condition=%wide.region_2.3_spmd.clone, body=%wide.region_1.2_spmd.clone.sunk | while | flops 131075 | bytes 656016 | solution.py:76
  52.0 13.9 %all-gather.1 = bf16[4,4,64,128]{3,2,1,0:T(8,128)(2,1)S(1)} all-gather(bf16[1,4,64,128]{3,2,1,0:T(8,128)(2,1)S(1)} %convert_element_type.121), channel_id=3, replica_groups=mesh['grp'=2,'sp'=4,'tp'=4] {'sp'}, dimensions={0}, use_global_device_ids=true | all-gather | bytes 327680 | tf_op jit(solution)/shard_map/all_gather | solution.py:16
  66.0 3.0 while.28
  68.9 2.8 fusion.32
  71.7 2.0 fusion.33
  74.6 5.7 %psum.7 = f32[256]{0:T(256)S(1)} all-reduce(f32[256]{0:T(256)S(1)} %multiply_reduce_fusion.1), channel_id=1, replica_groups=mesh['grp'=2,'sp'=4,'tp'=4] {'tp'}, use_global_device_ids=true, to_apply=%region_8.9 | all-reduce | flops 256 | bytes 2048 | tf_op jit(solution)/shard_map/psum | solution.py:165
  80.3 2.7 convolution_convert_fusion
  84.1 1.0 scatter_custom_fusion
  85.3 22.6 %reduce-scatter.5.cloned.1.call-done = bf16[64,2048]{1,0:T(8,128)(2,1)} async-done(((bf16[256,2048]{1,0:T(8,128)(2,1)}), bf16[64,2048]{1,0:T(8,128)(2,1)}) %reduce-scatter.5.cloned.1.call-update) | async-done | bytes 262160 | tf_op jit(solution)/shard_map/reduce_scatter | solution.py:171
  108.0 1.1 fusion.42
  109.1 1.1 fusion.44
  110.2 1.4 gather_fusion
  111.8 30.1 %all_to_all.10 = bf16[4,2,1,32,2048]{4,3,1,2,0:T(8,128)(2,1)} all-to-all(bf16[4,2,1,32,2048]{4,3,1,2,0:T(8,128)(2,1)S(1)} %select_select_fusion), channel_id=1, replica_groups=mesh['grp'=2,'sp'=4,'tp'=4] {'sp'}, dimensions={0} | all-to-all | bytes 2097152 | tf_op jit(solution)/shard_map/all_to_all | solution.py:195
  142.1 32.5 %all-gather.5.cloned.1.call-done = bf16[16,2,1,32,2048]{4,3,2,1,0:T(8,128)(2,1)} async-done(((bf16[4,2,1,32,2048]{4,3,2,1,0:T(8,128)(2,1)}), bf16[16,2,1,32,2048]{4,3,2,1,0:T(8,128)(2,1)}) %all-gather.5.cloned.1.call-update) | async-done | bytes 4194320 | tf_op jit(solution)/shard_map/all_gather | solution.py:196
  174.6 4.1 %fusion.12 = f32[4,2,4,32,256]{4,3,2,0,1:T(8,128)S(1)} fusion(bf16[2,2048,256]{2,1,0:T(8,128)(2,1)} %param.38, bf16[4,4,2,1,32,2048]{5,4,2,1,0,3:T(8,128)(2,1)} %bitcast.188), kind=kOutput, calls=%fused_computation.22 | convolution fusion | flops 1073741824 | bytes 7340032 | tf_op jit(solution)/shard_map/slqcd,ldf->slqcf/dot_general | solution.py:198
  178.8 7.3 %convert_bitcast_fusion = bf16[4,2,4,32,2048]{4,3,2,0,1:T(8,128)(2,1)} fusion(bf16[2,256,2048]{2,1,0:T(8,128)(2,1)S(1)} %copy-done, bf16[2,2048,256]{2,1,0:T(8,128)(2,1)} %param.39, bf16[4,4,2,1,32,2048]{5,4,2,1,0,3:T(8,128)(2,1)} %bitcast.189, f32[4,2,4,32,256]{4,3,2,0,1:T(8,128)S(1)} %fusion.12), kind=kOutput, calls=%fused_computation.15 | convolution fusion | flops 2151153664 | bytes 13631488 | tf_op jit(solution)/shard_map/slqcf,lfd->slqcd/dot_general | solution.py:205
  187.3 84.4 %all-reduce.4.cloned.1.call-done = bf16[4,2,4,32,2048]{4,3,2,0,1:T(8,128)(2,1)} async-done(((bf16[4,2,4,32,2048]{4,3,2,0,1:T(8,128)(2,1)}), bf16[4,2,4,32,2048]{4,3,2,0,1:T(8,128)(2,1)}) %all-reduce.4.cloned.1.call-update) | async-done | bytes 4194320
  271.7 1.9 constant_dynamic-slice_fusion.1
  273.7 1.1 copy.94
  274.7 4.7 %all-to-all-start.1 = ((bf16[4,2,1,32,2048]{4,3,2,1,0:T(8,128)(2,1)}), bf16[4,2,1,32,2048]{4,3,2,1,0:T(8,128)(2,1)S(1)}, u32[]{:S(2)}, u32[]{:S(2)}) async-start(bf16[4,2,1,32,2048]{4,3,2,1,0:T(8,128)(2,1)} %copy.94), calls=%async_computation.2 | async-start | bytes 2097152 | tf_op jit(solution)/shard_map/all_to_all | solution.py:211
  280.0 24.9 %all-to-all-done.1 = bf16[4,2,1,32,2048]{4,3,2,1,0:T(8,128)(2,1)S(1)} async-done(((bf16[4,2,1,32,2048]{4,3,2,1,0:T(8,128)(2,1)}), bf16[4,2,1,32,2048]{4,3,2,1,0:T(8,128)(2,1)S(1)}, u32[]{:S(2)}, u32[]{:S(2)}) %all-to-all-start.1) | async-done | bytes 1048608 | tf_op jit(solution)/shard_map/all_to_all | solution.py:211
  304.9 1.7 gather_fusion.1
  306.6 1.4 gather.15
  308.0 2.5 multiply_reduce_fusion
  310.5 1.8 fusion.45
  (118 shorter events, 27.3 us)
Async XLA Ops:
  6.5 172.2 %copy-start = (bf16[2,256,2048]{2,1,0:T(8,128)(2,1)S(1)}, bf16[2,256,2048]{2,1,0:T(8,128)(2,1)}, u32[]{:S(2)}) copy-start(bf16[2,256,2048]{2,1,0:T(8,128)(2,1)} %param.40) | copy-start | bytes 6291460
  6.5 101.4 %reduce-scatter.5.cloned.1.call-start = ((), (), s32[]{:S(2)}) async-start(), calls=%async_computation.3 | async-start | bytes 1310720 | tf_op jit(solution)/shard_map/reduce_scatter | solution.py:171
  7.4 35.9 %collective-permute-start.2 = (bf16[3,256]{1,0:T(4,128)(2,1)S(1)}, bf16[3,256]{1,0:T(4,128)(2,1)S(1)}, u32[]{:S(2)}, u32[]{:S(2)}) collective-permute-start(bf16[3,256]{1,0:T(4,128)(2,1)S(1)} %slice.103), channel_id=1, source_target_pairs={{0,4},{4,8},{8,12},{1,5},{5,9},{9,13},{2,6},{6,10},{10,14},{3,7},{... | collective-permute-start | bytes 4616 | tf_op jit(solution)/shard_map/ppermute | solution.py:35
  13.0 27.1 %collective-permute-start = (bf16[3,128]{1,0:T(4,128)(2,1)S(1)}, bf16[3,128]{1,0:T(4,128)(2,1)S(1)}, u32[]{:S(2)}, u32[]{:S(2)}) collective-permute-start(bf16[3,128]{1,0:T(4,128)(2,1)S(1)} %slice.85), channel_id=1, source_target_pairs={{0,4},{4,8},{8,12},{1,5},{5,9},{9,13},{2,6},{6,10},{10,14},{3,7},{... | collective-permute-start | bytes 2312 | tf_op jit(solution)/shard_map/ppermute | solution.py:35
  17.2 24.0 %collective-permute-start.1 = (bf16[3,128]{1,0:T(4,128)(2,1)S(1)}, bf16[3,128]{1,0:T(4,128)(2,1)S(1)}, u32[]{:S(2)}, u32[]{:S(2)}) collective-permute-start(bf16[3,128]{1,0:T(4,128)(2,1)S(1)} %slice.94), channel_id=1, source_target_pairs={{0,4},{4,8},{8,12},{1,5},{5,9},{9,13},{2,6},{6,10},{10,14},{3,7},{... | collective-permute-start | bytes 2312 | tf_op jit(solution)/shard_map/ppermute | solution.py:35
  41.1 1.0 copy-start.3
  52.0 22.5 %copy-start.4 = (bf16[256,256]{1,0:T(8,128)(2,1)S(1)}, bf16[256,256]{1,0:T(8,128)(2,1)}, u32[]{:S(2)}) copy-start(bf16[256,256]{1,0:T(8,128)(2,1)} %param.26) | copy-start | bytes 393220
  52.0 28.3 %copy-start.7 = (f32[256]{0:T(256)S(1)}, f32[256]{0:T(256)}, u32[]{:S(2)}) copy-start(f32[256]{0:T(256)} %dynamic_slice.31) | copy-start | bytes 3076
  68.9 14.2 %copy-start.8 = (s32[256,2]{0,1:T(2,128)S(1)}, s32[256,2]{0,1:T(2,128)}, u32[]{:S(2)}) copy-start(s32[256,2]{0,1:T(2,128)} %param.41) | copy-start | bytes 6148
  71.7 36.3 %copy-start.1 = (bf16[64,2048]{1,0:T(8,128)(2,1)S(1)}, bf16[64,2048]{1,0:T(8,128)(2,1)}, u32[]{:S(2)}) copy-start(bf16[64,2048]{1,0:T(8,128)(2,1)} %param.24) | copy-start | bytes 786436
  71.7 37.4 %copy-start.5 = (f32[2048]{0:T(1024)S(1)}, f32[2048]{0:T(1024)}, u32[]{:S(2)}) copy-start(f32[2048]{0:T(1024)} %param.37) | copy-start | bytes 24580
  83.1 91.6 %all-gather.5.cloned.1.call-start = ((), (), s32[]{:S(2)}) async-start(), calls=%async_computation.4 | async-start | bytes 5242880 | tf_op jit(solution)/shard_map/all_gather | solution.py:196
  141.9 129.8 %all-reduce.4.cloned.1.call-start = ((), (), s32[]{:S(2)}) async-start(), calls=%async_computation.5 | async-start | bytes 8388608
  186.1 0.7 copy-start.10
  186.1 93.7 %copy-start.6 = (f32[64,2]{0,1:T(2,128)S(1)}, f32[64,2]{0,1:T(2,128)}, u32[]{:S(2)}) copy-start(f32[64,2]{0,1:T(2,128)} %param.42) | copy-start | bytes 1540
  186.1 93.7 %copy-start.9 = (f32[64]{0:T(128)S(1)}, f32[64]{0:T(128)}, u32[]{:S(2)}) copy-start(f32[64]{0:T(128)} %param.43) | copy-start | bytes 772
  274.7 35.8 %copy-start.2 = (bf16[64,2048]{1,0:T(8,128)(2,1)S(1)}, bf16[64,2048]{1,0:T(8,128)(2,1)}, u32[]{:S(2)}) copy-start(bf16[64,2048]{1,0:T(8,128)(2,1)} %param.24) | copy-start | bytes 786436
  274.7 30.1 %all-to-all-start.1 = ((bf16[4,2,1,32,2048]{4,3,2,1,0:T(8,128)(2,1)}), bf16[4,2,1,32,2048]{4,3,2,1,0:T(8,128)(2,1)S(1)}, u32[]{:S(2)}, u32[]{:S(2)}) async-start(bf16[4,2,1,32,2048]{4,3,2,1,0:T(8,128)(2,1)} %copy.94), calls=%async_computation.2 | async-start | bytes 2097152 | tf_op jit(solution)/shard_map/all_to_all | solution.py:211
Sparse Core Ops, SparseCore 0:
  83.2 24.7 reduce-scatter.4
  142.0 32.5 all-gather.4
  186.2 85.4 all-reduce.3
